TPU v7x, 32 devices: a whole 2x2x4 slice. The times are simulated.
32 devices in a mesh: ep: 8 (over z, core), tp: 4 (over y, x).
Axes of the slice: x: 2, y: 2, z: 4, core: 2. Of those that a mesh axis runs over, the one named last changes fastest.
Arguments:
- mixer_value_input: bfloat16 [2048, 4096], P('ep', 'tp'), may hold values from -6 to 6
- input_state_matrix: bfloat16 [2048, 2048], P('ep', 'tp'), may hold values from -6 to 6
- output_state_matrix: bfloat16 [2048, 2048], P('ep', 'tp'), may hold values from -6 to 6
- output_gate_input: bfloat16 [2048, 4096], P('ep', 'tp'), may hold values from -6 to 6
- step_input: float32 [2048, 64], P('ep', 'tp'), may hold values from -6 to -2
- extra_log_decay: float32 [2048, 64], P('ep', 'tp'), may hold values from -1 to 0
- head_log_decay: float32 [64], P('tp'), may hold values from -10 to 1
- head_skip_scale: float32 [64], P('tp'), may hold values from 0.5 to 2
- value_kernel: float32 [4, 4096], P(None, 'tp'), may hold values from -3 to 3
- input_matrix_kernel: float32 [4, 2048], P(None, 'tp'), may hold values from -3 to 3
- output_matrix_kernel: float32 [4, 2048], P(None, 'tp'), may hold values from -3 to 3
- mixer_norm_scale: float32 [4096], P('tp'), may hold values from 0.1 to 1.9
- mixer_output_weight: bfloat16 [4096, 2048], P(None, 'tp'), may hold values from -0.09375 to 0.09375
- second_token_rows: bfloat16 [2048, 2048], P('ep'), may hold values from -6 to 6
- expert_norm_scale: float32 [2048], replicated, may hold values from 0.1 to 1.9
- routed_expert_index: int32 [2048, 4], P('ep'), may hold values from 0 to 15, all different within a row; in each aligned block of 256 rows (0 to 255, 256 to 511, ...) at most 96 rows name the same one
- routed_expert_weight: float32 [2048, 4], P('ep'), may hold values from 0.1 to 1
- routed_gate_weight: bfloat16 [16, 2048, 1024], P('ep', None, 'tp'), may hold values from -0.125 to 0.125
- routed_up_weight: bfloat16 [16, 2048, 1024], P('ep', None, 'tp'), may hold values from -0.125 to 0.125
- routed_down_weight: bfloat16 [16, 1024, 2048], P('ep', None, 'tp'), may hold values from -0.1875 to 0.1875
- shared_gate_weight: bfloat16 [2048, 1024], P(None, 'tp'), may hold values from -0.125 to 0.125
- shared_up_weight: bfloat16 [2048, 1024], P(None, 'tp'), may hold values from -0.125 to 0.125
- shared_down_weight: bfloat16 [1024, 2048], P(None, 'tp'), may hold values from -0.1875 to 0.1875
Outputs:
- mixer_output: bfloat16 [2048, 2048], P('ep', 'tp')
- routed_out: bfloat16 [2048, 2048], P('ep', 'tp')
Inputs may be any that keep to these rules, and one draw needn't show every extreme that they name: `routed_expert_index`: in each aligned block of 256 rows (the rows of one index of ep) no expert is named more than 96 times, a bound that some block reaches.
All inputs are finite; a program needn't handle non-finite values.
Results may differ from a plain program's by a relative error of at most 0.012.
Values may be sent and summed in bfloat16 or wider, within the bound.
A program may use at most 64 MiB of HBM per device.

v0:
```python
import jax
import jax.numpy as jnp
from jax import lax
from jax.sharding import PartitionSpec as P

HEAD_DIM = 64
STATE = 128
CONV_TAPS = 4
BLOCK = 128
TOP_K = 4
epsilon = 1e-05
precise = lax.Precision.HIGHEST


def passed_along(x, axis, by):
    size = lax.axis_size(axis)
    pairs = [(i, i + by) for i in range(size) if 0 <= i + by < size]
    return lax.ppermute(x, axis, pairs)


def carried_in(x, axis, join, neutral):
    place = lax.axis_index(axis)
    gathered = jax.tree.map(
        lambda a, kind: lax.all_gather(a.astype(kind), axis), x, (jnp.bfloat16, jnp.bfloat16)
    )
    state = jax.tree.map(lambda a, e: jnp.zeros_like(a) + jnp.asarray(e, a.dtype), x, neutral)

    def one(turn, state):
        return join(
            state,
            jax.tree.map(
                lambda a, own: lax.dynamic_index_in_dim(a, turn, 0, False).astype(own.dtype),
                gathered,
                x,
            ),
        )

    return lax.fori_loop(0, place, one, state)


def conv_silu(tail_rows, source, weights):
    length = source.shape[0]
    padded = jnp.concatenate([tail_rows, source], axis=0)
    total_sum = jnp.zeros(source.shape, jnp.float32)
    for tap_index in range(CONV_TAPS):
        total_sum = (
            total_sum
            + padded[tap_index : tap_index + length].astype(jnp.float32) * weights[tap_index]
        )
    return jax.nn.silu(total_sum).astype(jnp.bfloat16)


def join_states(earlier, later_part):
    return (earlier[0] * later_part[0], later_part[0][:, None, None] * earlier[1] + later_part[1])


def carry_blocks(carried, inputs):
    block_decay, block_state = inputs
    return (carried * block_decay[:, None, None] + block_state, carried)


def route_slots(route_block, experts, capacity):
    flat_ids = route_block.reshape(-1)
    onehot = (flat_ids[:, None] == jnp.arange(experts, dtype=jnp.int32)[None, :]).astype(jnp.int32)
    earlier = jnp.cumsum(onehot, axis=0) - onehot
    position_in = jnp.sum(earlier * onehot, axis=1)
    slot_index = flat_ids * capacity + position_in
    owner_row = jnp.arange(flat_ids.shape[0], dtype=jnp.int32) // route_block.shape[1]
    slot_owner = (
        jnp.full((experts * capacity,), route_block.shape[0], jnp.int32)
        .at[slot_index]
        .set(owner_row)
    )
    return (slot_owner, slot_index)


def on_device(
    mixer_value_input,
    input_state_matrix,
    output_state_matrix,
    output_gate_input,
    step_input,
    extra_log_decay,
    head_log_decay,
    head_skip_scale,
    value_kernel,
    input_matrix_kernel,
    output_matrix_kernel,
    mixer_norm_scale,
    mixer_output_weight,
    second_token_rows,
    expert_norm_scale,
    routed_expert_index,
    routed_expert_weight,
    routed_gate_weight,
    routed_up_weight,
    routed_down_weight,
    shared_gate_weight,
    shared_up_weight,
    shared_down_weight,
):
    length = mixer_value_input.shape[0]
    heads_local = step_input.shape[1]
    width_x = mixer_value_input.shape[1]
    width_b = input_state_matrix.shape[1]
    groups_local = width_b // STATE
    head_ratio = heads_local // groups_local
    nblocks = length // BLOCK
    lead_row = length - CONV_TAPS + 1
    edge_rows = jnp.concatenate(
        [
            mixer_value_input[lead_row:],
            input_state_matrix[lead_row:],
            output_state_matrix[lead_row:],
        ],
        axis=1,
    )
    tail_rows = passed_along(edge_rows, "ep", 1)
    values = conv_silu(tail_rows[:, :width_x], mixer_value_input, value_kernel)
    in_mat = conv_silu(
        tail_rows[:, width_x : width_x + width_b], input_state_matrix, input_matrix_kernel
    )
    out_mat = conv_silu(
        tail_rows[:, width_x + width_b :], output_state_matrix, output_matrix_kernel
    )
    step_length = jax.nn.softplus(step_input)
    decay_logarithm = -jnp.exp(head_log_decay)[None, :] * step_length + extra_log_decay
    running = jnp.cumsum(decay_logarithm.reshape(nblocks, BLOCK, heads_local), axis=1)
    value_wide = values.astype(jnp.float32).reshape(nblocks, BLOCK, heads_local, HEAD_DIM)
    scaled = value_wide * step_length.reshape(nblocks, BLOCK, heads_local)[..., None]
    in_blocks = in_mat.reshape(nblocks, BLOCK, groups_local, STATE)
    out_blocks = out_mat.reshape(nblocks, BLOCK, groups_local, STATE)
    scores = jnp.einsum(
        "bign,bjgn->bgij", out_blocks, in_blocks, preferred_element_type=jnp.float32
    )
    scores = jnp.repeat(scores, head_ratio, axis=1)
    spread = jnp.transpose(running[:, :, None, :] - running[:, None, :, :], (0, 3, 1, 2))
    lower_mask = jnp.tril(jnp.ones((BLOCK, BLOCK), bool))[None, None]
    decay_mat = jnp.where(lower_mask, jnp.exp(jnp.where(lower_mask, spread, 0.0)), 0.0)
    inside = jnp.einsum("bhij,bjhp->bihp", scores * decay_mat, scaled, precision=precise)
    out_head = jnp.repeat(out_blocks.astype(jnp.float32), head_ratio, axis=2)
    in_head = jnp.repeat(in_blocks.astype(jnp.float32), head_ratio, axis=2)
    block_logs = running[:, -1]
    to_end = jnp.exp(block_logs[:, None, :] - running)
    block_state = jnp.einsum("bjhn,bjh,bjhp->bhpn", in_head, to_end, scaled, precision=precise)
    start_state = jnp.zeros((heads_local, HEAD_DIM, STATE), jnp.float32)
    local_total, local_prev = lax.scan(
        carry_blocks, start_state, (jnp.exp(block_logs), block_state)
    )
    before_logs = jnp.cumsum(block_logs, axis=0) - block_logs
    incoming = carried_in(
        (jnp.exp(jnp.sum(block_logs, axis=0)), local_total),
        "ep",
        join_states,
        (jnp.ones((heads_local,), jnp.float32), start_state),
    )
    entering = local_prev + jnp.exp(before_logs)[:, :, None, None] * incoming[1][None]
    carried_term = (
        jnp.einsum("bihn,bhpn->bihp", out_head, entering, precision=precise)
        * jnp.exp(running)[..., None]
    )
    mixed_heads = (inside + carried_term).reshape(length, heads_local, HEAD_DIM)
    mixed_heads = mixed_heads + head_skip_scale[None, :, None] * value_wide.reshape(
        length, heads_local, HEAD_DIM
    )
    gated_heads = mixed_heads * jax.nn.silu(output_gate_input.astype(jnp.float32)).reshape(
        length, heads_local, HEAD_DIM
    )
    grouped = gated_heads.reshape(length, groups_local, head_ratio * HEAD_DIM)
    grouped = grouped * lax.rsqrt(jnp.mean(grouped * grouped, axis=-1, keepdims=True) + epsilon)
    mixer_normed = (grouped.reshape(length, width_x) * mixer_norm_scale).astype(jnp.bfloat16)
    rows_local = second_token_rows.shape[0]
    model_width = second_token_rows.shape[1]
    local_experts = routed_gate_weight.shape[0]
    ep_count = lax.axis_size("ep")
    experts = local_experts * ep_count
    capacity = max(2, 3 * rows_local * TOP_K // (2 * experts))
    col_width = model_width // lax.axis_size("tp")
    rows_wide = second_token_rows.astype(jnp.float32)
    normed = (
        rows_wide
        * lax.rsqrt(jnp.mean(rows_wide * rows_wide, axis=-1, keepdims=True) + epsilon)
        * expert_norm_scale
    ).astype(jnp.bfloat16)
    slot_owner, slot_index = route_slots(routed_expert_index, experts, capacity)
    padded = jnp.concatenate([normed, jnp.zeros((1, model_width), jnp.bfloat16)], axis=0)
    outgoing = jnp.take(padded, slot_owner, axis=0).reshape(experts, capacity, model_width)
    my_columns = lax.dynamic_slice_in_dim(outgoing, lax.axis_index("tp") * col_width, col_width, 2)
    arrived = lax.all_to_all(my_columns, "ep", split_axis=0, concat_axis=1, tiled=True)
    column_piece = lax.all_gather(arrived, "tp", axis=2, tiled=True)
    gate_pre = jnp.einsum(
        "esd,edf->esf", column_piece, routed_gate_weight, preferred_element_type=jnp.float32
    )
    up_pre = jnp.einsum(
        "esd,edf->esf", column_piece, routed_up_weight, preferred_element_type=jnp.float32
    )
    hidden = (jax.nn.silu(gate_pre) * up_pre).astype(jnp.bfloat16)
    shared_hidden = (
        jax.nn.silu(jnp.dot(normed, shared_gate_weight, preferred_element_type=jnp.float32))
        * jnp.dot(normed, shared_up_weight, preferred_element_type=jnp.float32)
    ).astype(jnp.bfloat16)
    whole_mix, whole_hidden, whole_shared = (
        lax.all_gather(mixer_normed, "tp", axis=1, tiled=True),
        lax.all_gather(hidden, "tp", axis=2, tiled=True),
        lax.all_gather(shared_hidden, "tp", axis=1, tiled=True),
    )
    mixer_output = jnp.dot(
        whole_mix, mixer_output_weight, preferred_element_type=jnp.float32
    ).astype(jnp.bfloat16)
    expert_result = jnp.einsum(
        "esf,efd->esd", whole_hidden, routed_down_weight, preferred_element_type=jnp.float32
    ).astype(jnp.bfloat16)
    returned = lax.all_to_all(expert_result, "ep", split_axis=1, concat_axis=0, tiled=True)
    picked = jnp.take(returned.reshape(experts * capacity, col_width), slot_index, axis=0)
    picked = picked.reshape(rows_local, TOP_K, col_width).astype(jnp.float32)
    routed_sum = jnp.sum(picked * routed_expert_weight[:, :, None], axis=1)
    shared_result = jnp.dot(whole_shared, shared_down_weight, preferred_element_type=jnp.float32)
    routed_out = (routed_sum + shared_result).astype(jnp.bfloat16)
    return (mixer_output, routed_out)


def solution(mesh):
    return jax.shard_map(
        on_device,
        mesh=mesh,
        in_specs=(
            P("ep", "tp"),
            P("ep", "tp"),
            P("ep", "tp"),
            P("ep", "tp"),
            P("ep", "tp"),
            P("ep", "tp"),
            P("tp"),
            P("tp"),
            P(None, "tp"),
            P(None, "tp"),
            P(None, "tp"),
            P("tp"),
            P(None, "tp"),
            P("ep", None),
            P(),
            P("ep", None),
            P("ep", None),
            P("ep", None, "tp"),
            P("ep", None, "tp"),
            P("ep", None, "tp"),
            P(None, "tp"),
            P(None, "tp"),
            P(None, "tp"),
        ),
        out_specs=(P("ep", "tp"), P("ep", "tp")),
        check_vma=False,
    )
```

profile of v0, /device:TPU:0, one launch (start us, length us, event | category | flops | bytes accessed | tf_op | source)
XLA Modules:
  0.0 292.6 jit_solution(14076036180507357092)
XLA Ops:
  7.2 1.0 copy.117
  8.5 0.7 broadcast_multiply_fusion.2
  9.2 4.5 %reduce-window.6 = s32[16,8,128]{2,1,0:T(8,128)S(1)} reduce-window(s32[16,8,128]{2,1,0:T(8,128)S(1)} %fusion.50, s32[]{:T(128)} %constant.114.clone.1), window={size=1x1x128 pad=0_0x0_0x127_0}, to_apply=%region_8.9 | reduce-window | flops 2080768 | bytes 131076 | tf_op jit(solution)/shard_map/reduce-window
  15.6 4.3 %scatter_custom_fusion = s32[1536]{0:T(1024)S(1)} fusion(s32[1024]{0:T(1024)S(1)} %bitcast.142, s32[1024]{0:T(1024)S(1)} %add_select_fusion, s32[]{:T(128)} %constant.122.clone.1), kind=kCustom, calls=%fused_computation.105 | custom fusion | bytes 6148 | tf_op jit(solution)/shard_map/scatter | solution.py:72
  20.7 1.0 copy-done.2
  21.7 7.0 %gather_fusion = bf16[1536,2048]{1,0:T(8,128)(2,1)} fusion(bf16[257,2048]{1,0:T(8,128)(2,1)S(1)} %concatenate.19, s32[2048]{0:T(1024)S(1)} %pad_clamp_fusion), kind=kCustom, calls=%fused_computation | custom fusion | bytes 12589056 | tf_op jit(solution)/shard_map/jit(_take)/gather | solution.py:187
  28.8 1.8 dynamic-slice_select_fusion
  30.6 43.9 %all_to_all.33 = bf16[16,96,512]{2,1,0:T(8,128)(2,1)S(1)} all-to-all(bf16[16,96,512]{2,1,0:T(8,128)(2,1)S(1)} %dynamic-slice_select_fusion), channel_id=1, replica_groups=mesh['ep'=8,'tp'=4] {'ep'}, dimensions={0} | all-to-all | bytes 3145728 | tf_op jit(solution)/shard_map/all_to_all | solution.py:189
  74.5 1.3 copy.124
  75.9 0.7 slice.91
  76.6 0.7 slice.92
  77.3 1.0 copy.98
  78.4 2.2 collective-permute-start
  80.6 0.6 compare_select_fusion
  82.7 0.6 fusion.59
  84.3 1.3 mul.329
  85.6 1.0 slice.124
  86.6 2.9 fusion.39
  89.5 2.7 reshape.196
  92.2 1.0 fusion.57
  93.3 1.9 multiply_convert_fusion.2
  95.4 2.9 broadcast_multiply_fusion
  98.5 3.1 %fusion.26 = f32[2,16,64,128]{3,2,1,0:T(8,128)} fusion(f32[2,128,16,128]{3,1,2,0:T(8,128)S(1)} %bitcast.125, f32[2,128,16,64]{1,0,3,2:T(2,128)S(1)} %get-tuple-element.115), kind=kOutput, calls=%fused_computation.43 | convolution fusion | flops 402653184 | bytes 4194304 | tf_op jit(solution)/shard_map/bjhn,bjh,bjhp->bhpn/dot_general | solution.py:145
  101.6 4.1 %while.26 = (s32[]{:T(128)}, f32[16,64,128]{2,1,0:T(8,128)S(1)}, f32[2,16,64,128]{3,2,1,0:T(8,128)}, f32[2,16]{1,0:T(2,128)S(1)}, f32[2,16,64,128]{3,2,1,0:T(8,128)}, /*index=5*/s32[]{:T(128)}, s32[]{:T(128)}) while((s32[]{:T(128)}, f32[16,64,128]{2,1,0:T(8,128)S(1)}, f32[2,16,64,128]{3,2,1,0:T(8,128)}, f32[2,16]{1,0:T(2,128)S(1)}, ...), condition=%wide.region_2.3_spmd.clone, body=%wide.region_1.2_spmd.clone.sunk | while | flops 524291 | bytes 2622240 | solution.py:147
  101.6 0.9 bitcast_dynamic-update-slice_fusion.2
  102.5 1.2 bitcast_add_fusion.3
  103.6 0.9 bitcast_dynamic-update-slice_fusion.2
  104.5 1.2 bitcast_add_fusion.3
  105.7 0.7 convert_element_type.144
  106.7 38.1 %all-gather.9.cloned.1.call-done = bf16[2,768,2048]{2,1,0:T(8,128)(2,1)} async-done(((bf16[2,768,512]{2,1,0:T(8,128)(2,1)}), bf16[2,768,2048]{2,1,0:T(8,128)(2,1)}) %all-gather.9.cloned.1.call-update) | async-done | bytes 6291472 | tf_op jit(solution)/shard_map/all_gather | solution.py:190
  144.8 5.3 %fusion.62 = f32[2,768,256]{2,1,0:T(8,128)S(1)} fusion(bf16[2,768,2048]{2,1,0:T(8,128)(2,1)} %all-gather.9.cloned.1.call-done, bf16[2,2048,256]{2,1,0:T(8,128)(2,1)} %param.44), kind=kOutput, calls=%fused_computation.123 | convolution fusion | flops 1610612736 | bytes 9961472 | tf_op jit(solution)/shard_map/esd,edf->esf/dot_general | solution.py:191
  150.7 2.9 multiply_convert_fusion
  153.8 0.7 mul.373
  154.5 0.7 mul.368
  155.2 1.2 dynamic-slice
  157.3 17.1 %all-reduce.1 = bf16[128]{0:T(256)(128)(2,1)S(1)} all-reduce(bf16[128]{0:T(256)(128)(2,1)S(1)} %dynamic-update-slice), channel_id=2, replica_groups=mesh['ep'=8,'tp'=4] {'ep'}, use_global_device_ids=true, to_apply=%add.1 | all-reduce | flops 128 | bytes 512
  174.5 0.7 reshape.235
  175.2 0.7 copy.113
  175.9 1.1 copy.115
  177.0 0.6 iota_compare_fusion.2
  177.6 0.9 fusion.61
  179.0 0.8 copy.112
  180.2 1.4 broadcast_in_dim.92
  181.6 4.2 %fusion.16 = f32[2,128,16,64]{1,3,2,0:T(8,128)S(1)} fusion(f32[2,128,16,128]{3,1,2,0:T(8,128)S(1)} %bitcast.126, f32[2,16,64,128]{3,2,1,0:T(8,128)S(1)} %copy-done.9, f32[2,128,16]{1,2,0:T(8,128)S(1)} %copy-done.14, f32[16,64,128]{2,1,0:T(8,128)S(1)} %get-tuple-element.76, f32[2,16]{1,0:T(2,128)S(1)} %copy-done.33), kind=kOutput, calls=%fused_computation.27 | convolution fusion | flops 403439616 | bytes 4735104 | tf_op jit(solution)/shard_map/bihn,bhpn->bihp/dot_general | solution.py:159
  186.1 1.0 copy-done.6
  187.1 4.2 %fusion.13 = f32[2,128,16,64]{1,3,2,0:T(8,128)S(1)} fusion(f32[2,128,16,64]{1,3,2,0:T(8,128)S(1)} %fusion.16, f32[2,16,128,128]{3,2,1,0:T(8,128)S(1)} %bitcast.124, f32[2,128,16,64]{1,0,3,2:T(2,128)S(1)} %copy-done.6, f32[2,16,128]{2,1,0:T(8,128)S(1)} %copy.106, pred[128,128]{1,0:T(8,128)(4,1)S(1)} %copy-done.13), kind=kOutput, calls=%fused_computation.25 | convolution fusion | flops 405012480 | bytes 5275648 | tf_op jit(solution)/shard_map/bhij,bjhp->bihp/dot_general | solution.py:140
  191.3 1.8 copy.114
  193.1 3.1 %reshape.204 = f32[256,4,256]{0,2,1:T(8,128)} reshape(f32[2,128,16,64]{1,0,3,2:T(2,128)} %copy.114) | data formatting | bytes 2097152 | tf_op jit(solution)/shard_map/reshape | solution.py:162
  196.3 1.9 multiply_reduce_fusion.1
  198.2 1.3 fusion.25
  199.6 21.9 %all-gather.11.cloned.1.call-done = bf16[2,768,1024]{2,1,0:T(8,128)(2,1)} async-done(((bf16[2,768,256]{2,1,0:T(8,128)(2,1)}), bf16[2,768,1024]{2,1,0:T(8,128)(2,1)}) %all-gather.11.cloned.1.call-update) | async-done | bytes 3145744 | tf_op jit(solution)/shard_map/all_gather | solution.py:204
  221.5 3.7 %convolution_convert_fusion = bf16[2,768,512]{2,1,0:T(8,128)(2,1)S(1)} fusion(bf16[2,768,1024]{2,1,0:T(8,128)(2,1)} %all-gather.11.cloned.1.call-done, bf16[2,1024,512]{2,1,0:T(8,128)(2,1)S(1)} %copy-done), kind=kOutput, calls=%fused_computation.21 | convolution fusion | flops 1611399168 | bytes 6815744 | tf_op jit(solution)/shard_map/esf,efd->esd/dot_general | solution.py:210
  225.2 2.8 copy.125
  227.9 5.0 %all-to-all-start.1 = ((bf16[2,768,512]{2,0,1:T(2,128)(2,1)}), bf16[2,768,512]{2,0,1:T(2,128)(2,1)}, u32[]{:S(2)}, u32[]{:S(2)}) async-start(bf16[2,768,512]{2,0,1:T(2,128)(2,1)} %copy.125), calls=%async_computation.1 | async-start | bytes 3145728 | tf_op jit(solution)/shard_map/all_to_all | solution.py:213
  233.5 1.7 fusion.63
  235.7 20.6 %all_gather.28 = bf16[256,1024]{1,0:T(8,128)(2,1)} all-gather(bf16[256,256]{1,0:T(8,128)(2,1)S(1)} %fusion.18), channel_id=1, replica_groups=mesh['ep'=8,'tp'=4] {'tp'}, dimensions={1}, use_global_device_ids=true | all-gather | bytes 655360 | tf_op jit(solution)/shard_map/all_gather | solution.py:205
  256.3 6.2 %all-gather.7.cloned.1.call-done = bf16[256,4096]{0,1:T(8,128)(2,1)} async-done(((bf16[256,1024]{0,1:T(8,128)(2,1)}), bf16[256,4096]{0,1:T(8,128)(2,1)}) %all-gather.7.cloned.1.call-update) | async-done | bytes 2097168 | tf_op jit(solution)/shard_map/all_gather | solution.py:203
  262.6 4.8 %convolution_convert_fusion.1 = bf16[256,512]{1,0:T(8,128)(2,1)} fusion(bf16[256,4096]{0,1:T(8,128)(2,1)} %all-gather.7.cloned.1.call-done, bf16[4096,512]{1,0:T(8,128)(2,1)} %param.39), kind=kOutput, calls=%fused_computation.32 | convolution fusion | flops 1073872896 | bytes 6553600 | tf_op jit(solution)/shard_map/dot_general | solution.py:207
  267.3 3.5 %all-to-all-done.1 = bf16[2,768,512]{2,0,1:T(2,128)(2,1)} async-done(((bf16[2,768,512]{2,0,1:T(2,128)(2,1)}), bf16[2,768,512]{2,0,1:T(2,128)(2,1)}, u32[]{:S(2)}, u32[]{:S(2)}) %all-to-all-start.1) | async-done | bytes 1572896 | tf_op jit(solution)/shard_map/all_to_all | solution.py:213
  270.8 2.9 copy.126
  273.7 5.6 %gather_fusion.1 = bf16[1024,512]{1,0:T(8,128)(2,1)S(1)} fusion(bf16[1536,512]{1,0:T(8,128)(2,1)} %bitcast.121, s32[1024]{0:T(1024)S(1)} %broadcast_clamp_fusion), kind=kCustom, calls=%fused_computation.1 | custom fusion | bytes 2101248 | tf_op jit(solution)/shard_map/jit(_take)/gather | solution.py:214
  279.3 1.1 gather.15
  280.4 3.4 %multiply_reduce_fusion = f32[256,512]{1,0:T(8,128)S(1)} fusion(f32[256,4]{1,0:T(8,128)S(1)} %copy.127, bf16[256,4,512]{2,1,0:T(4,128)(2,1)} %gather.15, pred[256,4]{1,0:T(8,128)(4,1)S(1)} %copy.122), kind=kLoop, calls=%fused_computation.14 | loop fusion | flops 1966080 | bytes 1577984 | tf_op jit(solution)/shard_map/reduce_sum | solution.py:216
  283.9 2.2 fusion.17
  (153 shorter events, 9.4 us)
Async XLA Ops:
  7.2 214.3 %copy-start = (bf16[2,1024,512]{2,1,0:T(8,128)(2,1)S(1)}, bf16[2,1024,512]{2,1,0:T(8,128)(2,1)}, u32[]{:S(2)}) copy-start(bf16[2,1024,512]{2,1,0:T(8,128)(2,1)} %param.46) | copy-start | bytes 6291460
  7.2 12.8 %copy-start.7 = (bf16[256,2048]{1,0:T(8,128)(2,1)S(1)}, bf16[256,2048]{1,0:T(8,128)(2,1)}, u32[]{:S(2)}) copy-start(bf16[256,2048]{1,0:T(8,128)(2,1)} %param.40) | copy-start | bytes 3145732
  7.2 13.2 %copy-start.25 = (f32[2048]{0:T(1024)S(1)}, f32[2048]{0:T(1024)}, u32[]{:S(2)}) copy-start(f32[2048]{0:T(1024)} %param.41) | copy-start | bytes 24580
  7.2 137.6 %all-gather.9.cloned.1.call-start = ((), (), s32[]{:S(2)}) async-start(), calls=%async_computation.3 | async-start | bytes 7864320 | tf_op jit(solution)/shard_map/all_gather | solution.py:190
  14.4 0.6 copy-start.15
  15.0 0.6 copy-start.20
  20.7 1.0 copy-start.2
  74.5 1.4 copy-start.10
  74.5 6.0 %copy-start.40 = (f32[16]{0:T(128)S(1)}, f32[16]{0:T(128)}, u32[]{:S(2)}) copy-start(f32[16]{0:T(128)} %param.33) | copy-start | bytes 196
  74.5 6.0 %copy-start.23 = (f32[256,16]{0,1:T(8,128)S(1)}, f32[256,16]{0,1:T(8,128)}, u32[]{:S(2)}) copy-start(f32[256,16]{0,1:T(8,128)} %param.31) | copy-start | bytes 49156
  74.5 6.0 %copy-start.24 = (f32[256,16]{0,1:T(8,128)S(1)}, f32[256,16]{0,1:T(8,128)}, u32[]{:S(2)}) copy-start(f32[256,16]{0,1:T(8,128)} %param.32) | copy-start | bytes 49156
  75.8 6.3 %copy-start.30 = (f32[4,512]{1,0:T(4,128)S(1)}, f32[4,512]{1,0:T(4,128)}, u32[]{:S(2)}) copy-start(f32[4,512]{1,0:T(4,128)} %param.36) | copy-start | bytes 24580
  75.8 6.9 %copy-start.22 = (f32[4,1024]{1,0:T(4,128)S(1)}, f32[4,1024]{1,0:T(4,128)}, u32[]{:S(2)}) copy-start(f32[4,1024]{1,0:T(4,128)} %param.35) | copy-start | bytes 49156
  75.8 104.3 %all-gather.13.cloned.1.call-start = ((), (), s32[]{:S(2)}) async-start(), calls=%async_computation.5 | async-start | bytes 2359296 | tf_op jit(solution)/shard_map/all_gather | solution.py:24
  78.4 7.2 %collective-permute-start = (bf16[3,2048]{0,1:T(8,128)(2,1)}, bf16[3,2048]{0,1:T(8,128)(2,1)}, u32[]{:S(2)}, u32[]{:S(2)}) collective-permute-start(bf16[3,2048]{0,1:T(8,128)(2,1)} %copy.98), channel_id=1, source_target_pairs={{0,4},{4,8},{8,12},{12,16},{16,20},{20,24},{24,28},{1,5},{5,9},{9,... | collective-permute-start | bytes 36872 | tf_op jit(solution)/shard_map/ppermute | solution.py:18
  89.5 3.8 %copy-start.26 = (f32[1,512]{1,0:T(1,128)S(1)}, f32[1,512]{1,0:T(1,128)}, u32[]{:S(2)}) copy-start(f32[1,512]{1,0:T(1,128)} %get-tuple-element.129) | copy-start | bytes 6148
  89.5 3.8 %copy-start.27 = (f32[1,512]{1,0:T(1,128)S(1)}, f32[1,512]{1,0:T(1,128)}, u32[]{:S(2)}) copy-start(f32[1,512]{1,0:T(1,128)} %get-tuple-element.130) | copy-start | bytes 6148
  89.5 3.8 %copy-start.28 = (f32[1,512]{1,0:T(1,128)S(1)}, f32[1,512]{1,0:T(1,128)}, u32[]{:S(2)}) copy-start(f32[1,512]{1,0:T(1,128)} %get-tuple-element.131) | copy-start | bytes 6148
  89.5 3.8 %copy-start.29 = (f32[1,512]{1,0:T(1,128)S(1)}, f32[1,512]{1,0:T(1,128)}, u32[]{:S(2)}) copy-start(f32[1,512]{1,0:T(1,128)} %get-tuple-element.132) | copy-start | bytes 6148
  98.5 3.1 %copy-start.34 = (f32[2,16]{1,0:T(2,128)S(1)}, f32[2,16]{1,0:T(2,128)}, u32[]{:S(2)}) copy-start(f32[2,16]{1,0:T(2,128)} %get-tuple-element.205) | copy-start | bytes 388
  106.5 115.0 %all-gather.11.cloned.1.call-start = ((), (), s32[]{:S(2)}) async-start(), calls=%async_computation.4 | async-start | bytes 3932160 | tf_op jit(solution)/shard_map/all_gather | solution.py:204
  144.8 5.4 %copy-start.37 = (bf16[2,768,2048]{2,1,0:T(8,128)(2,1)S(1)}, bf16[2,768,2048]{2,1,0:T(8,128)(2,1)}, u32[]{:S(2)}) copy-start(bf16[2,768,2048]{2,1,0:T(8,128)(2,1)} %all-gather.9.cloned.1.call-done) | copy-start | bytes 18874372
  144.8 5.8 %copy-start.38 = (bf16[2,2048,256]{2,1,0:T(8,128)(2,1)S(1)}, bf16[2,2048,256]{2,1,0:T(8,128)(2,1)}, u32[]{:S(2)}) copy-start(bf16[2,2048,256]{2,1,0:T(8,128)(2,1)} %param.45) | copy-start | bytes 6291460
  150.7 3.0 %copy-start.35 = (f32[16]{0:T(128)S(1)}, f32[16]{0:T(128)}, u32[]{:S(2)}) copy-start(f32[16]{0:T(128)} %param.34) | copy-start | bytes 196
  150.7 6.4 %copy-start.36 = (f32[16]{0:T(128)S(1)}, f32[16]{0:T(128)}, u32[]{:S(2)}) copy-start(f32[16]{0:T(128)} %get-tuple-element.119) | copy-start | bytes 196
  150.7 25.2 %copy-start.11 = (bf16[256,1024]{1,0:T(8,128)(2,1)S(1)}, bf16[256,1024]{1,0:T(8,128)(2,1)}, u32[]{:S(2)}) copy-start(bf16[256,1024]{1,0:T(8,128)(2,1)} %param.30) | copy-start | bytes 1572868
  153.6 25.0 %copy-start.12 = (bf16[256,512]{1,0:T(8,128)(2,1)S(1)}, bf16[256,512]{1,0:T(8,128)(2,1)}, u32[]{:S(2)}) copy-start(bf16[256,512]{1,0:T(8,128)(2,1)} %param.29) | copy-start | bytes 786436
  153.6 109.0 %all-gather.7.cloned.1.call-start = ((), (), s32[]{:S(2)}) async-start(), calls=%async_computation.2 | async-start | bytes 2621440 | tf_op jit(solution)/shard_map/all_gather | solution.py:203
  180.2 1.4 copy-start.9
  180.2 1.4 copy-start.14
  180.2 1.4 copy-start.33
  185.8 1.3 copy-start.6
  185.8 1.3 copy-start.13
  191.3 4.9 %copy-start.1 = (f32[256,1024]{0,1:T(8,128)S(1)}, f32[256,1024]{0,1:T(8,128)}, u32[]{:S(2)}) copy-start(f32[256,1024]{0,1:T(8,128)} %fusion.39) | copy-start | bytes 3145732
  191.3 4.9 %copy-start.19 = (f32[4,256]{1,0:T(4,128)S(1)}, f32[4,256]{1,0:T(4,128)}, u32[]{:S(2)}) copy-start(f32[4,256]{1,0:T(4,128)} %mul.373) | copy-start | bytes 12292
  193.1 5.1 %copy-start.18 = (f32[1024]{0:T(1024)S(1)}, f32[1024]{0:T(1024)}, u32[]{:S(2)}) copy-start(f32[1024]{0:T(1024)} %mul.368) | copy-start | bytes 12292
  193.1 5.1 %copy-start.31 = (f32[1024]{0:T(1024)S(1)}, f32[1024]{0:T(1024)}, u32[]{:S(2)}) copy-start(f32[1024]{0:T(1024)} %param.38) | copy-start | bytes 12292
  196.3 2.0 copy-start.4
  196.3 2.0 copy-start.5
  227.9 5.0 %copy-start.16 = (s32[1024]{0:T(1024)S(1)}, s32[1024]{0:T(1024)}, u32[]{:S(2)}) copy-start(s32[1024]{0:T(1024)} %copy-done.15) | copy-start | bytes 12292
  227.9 5.2 %copy-start.17 = (s32[256,4]{0,1:T(4,128)S(1)}, s32[256,4]{0,1:T(4,128)}, u32[]{:S(2)}) copy-start(s32[256,4]{0,1:T(4,128)} %param.42) | copy-start | bytes 12292
  227.9 5.4 %copy-start.32 = (f32[256,4]{0,1:T(4,128)S(1)}, f32[256,4]{0,1:T(4,128)}, u32[]{:S(2)}) copy-start(f32[256,4]{0,1:T(4,128)} %param.43) | copy-start | bytes 12292
  227.9 5.6 %copy-start.3 = (bf16[256,2048]{1,0:T(8,128)(2,1)S(1)}, bf16[256,2048]{1,0:T(8,128)(2,1)}, u32[]{:S(2)}) copy-start(bf16[256,2048]{1,0:T(8,128)(2,1)} %copy-done.2) | copy-start | bytes 3145732
  227.9 42.9 %all-to-all-start.1 = ((bf16[2,768,512]{2,0,1:T(2,128)(2,1)}), bf16[2,768,512]{2,0,1:T(2,128)(2,1)}, u32[]{:S(2)}, u32[]{:S(2)}) async-start(bf16[2,768,512]{2,0,1:T(2,128)(2,1)} %copy.125), calls=%async_computation.1 | async-start | bytes 3145728 | tf_op jit(solution)/shard_map/all_to_all | solution.py:213
  233.5 1.8 copy-start.39
  235.3 21.0 %copy-start.21 = (s32[1024,1]{0,1:T(1,128)S(1)}, s32[1024,1]{0,1:T(1,128)}, u32[]{:S(2)}) copy-start(s32[1024,1]{0,1:T(1,128)} %copy-done.20) | copy-start | bytes 12292
  280.4 3.4 %copy-start.8 = (bf16[1024,512]{1,0:T(8,128)(2,1)S(1)}, bf16[1024,512]{1,0:T(8,128)(2,1)}, u32[]{:S(2)}) copy-start(bf16[1024,512]{1,0:T(8,128)(2,1)} %param.49) | copy-start | bytes 3145732
Sparse Core Ops, SparseCore 0:
  76.0 68.8 all-gather.8
  147.0 29.4 all-gather.12
  178.3 43.1 all-gather.10
  223.2 39.3 all-gather.6
where the time goes:
time: 294 us; the launch traced here: 293 us
  blocking collectives  81.7 us (28%)
  waiting for transfers between devices  69.8 us (24%)
  local copies, waits for them, and re-layouts  55.5 us (19%)
  matrix products  32.9 us (11%)
  other arithmetic  30 us (10%)
  between operations  15.1 us (5%)
  starting transfers between devices  7.51 us (3%)
    all_to_all x1, blocking collectives, on_device(): lax.all_to_all(my_columns, 'ep', split_axis=0, concat_axis=1, tiled=True)  43.9 us
    all_gather x1, waiting for transfers between devices, on_device(): column_piece = lax.all_gather(arrived, 'tp', axis=2, tiled=True)  38.1 us
    all_gather x1, waiting for transfers between devices, on_device(): lax.all_gather(hidden, 'tp', axis=2, tiled=True)  21.9 us
    all_gather x1, blocking collectives, on_device(): lax.all_gather(shared_hidden, 'tp', axis=1, tiled=True)  20.6 us
    unnamed x1, blocking collectives  17.1 us
    unnamed x89, local copies, waits for them, and re-layouts  7.6 us
    gather x1, local copies, waits for them, and re-layouts, on_device(): jnp.take(padded, slot_owner, axis=0).reshape(experts, capacity, model_width)  7.02 us
    gather x2, local copies, waits for them, and re-layouts, on_device(): jnp.take(returned.reshape(experts * capacity, col_width), slot_index, axi...  6.73 us
  transfers between devices with their start and end apart: 6, of which 4 were waited for; matrix products, arithmetic and copies ran while one was open for 26% of the time, Pallas kernels for 0%

commit v1 on v0

--- a/solution.py
+++ b/solution.py
@@ -186,7 +186,10 @@
     padded = jnp.concatenate([normed, jnp.zeros((1, model_width), jnp.bfloat16)], axis=0)
     outgoing = jnp.take(padded, slot_owner, axis=0).reshape(experts, capacity, model_width)
     my_columns = lax.dynamic_slice_in_dim(outgoing, lax.axis_index("tp") * col_width, col_width, 2)
-    arrived = lax.all_to_all(my_columns, "ep", split_axis=0, concat_axis=1, tiled=True)
+    arrived = jnp.concatenate(
+        lax.all_to_all(jnp.stack(jnp.split(my_columns, lax.axis_size("ep"), axis=0)), "ep", 0, 0),
+        axis=1,
+    )
     column_piece = lax.all_gather(arrived, "tp", axis=2, tiled=True)
     gate_pre = jnp.einsum(
         "esd,edf->esf", column_piece, routed_gate_weight, preferred_element_type=jnp.float32

time: 294 us -> 294 us (level)
    unnamed x89 -> x96, local copies, waits for them, and re-layouts: 7.6 us -> 7.71 us
where the time goes in v1:
time: 294 us; the launch traced here: 293 us
  blocking collectives  81.7 us (28%)
  waiting for transfers between devices  69.8 us (24%)
  local copies, waits for them, and re-layouts  55.6 us (19%)
  matrix products  32.9 us (11%)
  other arithmetic  30 us (10%)
  between operations  15.2 us (5%)
  starting transfers between devices  7.48 us (3%)
    all_to_all x1, blocking collectives, on_device(): lax.all_to_all(jnp.stack(jnp.split(my_columns, lax.axis_size('ep'), axis=...  43.9 us
    all_gather x1, waiting for transfers between devices, on_device(): column_piece = lax.all_gather(arrived, 'tp', axis=2, tiled=True)  38.1 us
    all_gather x1, waiting for transfers between devices, on_device(): lax.all_gather(hidden, 'tp', axis=2, tiled=True)  21.9 us
    all_gather x1, blocking collectives, on_device(): lax.all_gather(shared_hidden, 'tp', axis=1, tiled=True)  20.6 us
    unnamed x1, blocking collectives  17.2 us
    unnamed x96, local copies, waits for them, and re-layouts  7.71 us
    gather x1, local copies, waits for them, and re-layouts, on_device(): jnp.take(padded, slot_owner, axis=0).reshape(experts, capacity, model_width)  7.02 us
    gather x2, local copies, waits for them, and re-layouts, on_device(): jnp.take(returned.reshape(experts * capacity, col_width), slot_index, axi...  6.73 us
  transfers between devices with their start and end apart: 6, of which 4 were waited for; matrix products, arithmetic and copies ran while one was open for 26% of the time, Pallas kernels for 0%

profile of v1, /device:TPU:0, one launch (start us, length us, event | category | flops | bytes accessed | tf_op | source)
XLA Modules:
  0.0 292.8 jit_solution(6314324733362054698)
XLA Ops:
  7.2 1.0 copy.130
  8.5 0.7 broadcast_multiply_fusion.2
  9.2 4.5 %reduce-window.6 = s32[16,8,128]{2,1,0:T(8,128)S(1)} reduce-window(s32[16,8,128]{2,1,0:T(8,128)S(1)} %fusion.58, s32[]{:T(128)} %constant.114.clone.1), window={size=1x1x128 pad=0_0x0_0x127_0}, to_apply=%region_8.9 | reduce-window | flops 2080768 | bytes 131076 | tf_op jit(solution)/shard_map/reduce-window
  15.6 4.3 %scatter_custom_fusion = s32[1536]{0:T(1024)S(1)} fusion(s32[1024]{0:T(1024)S(1)} %bitcast.172, s32[1024]{0:T(1024)S(1)} %add_select_fusion, s32[]{:T(128)} %constant.122.clone.1), kind=kCustom, calls=%fused_computation.121 | custom fusion | bytes 6148 | tf_op jit(solution)/shard_map/scatter | solution.py:72
  20.7 1.0 copy-done.2
  21.7 7.0 %gather_fusion = bf16[1536,2048]{1,0:T(8,128)(2,1)} fusion(bf16[257,2048]{1,0:T(8,128)(2,1)S(1)} %concatenate.19, s32[2048]{0:T(1024)S(1)} %pad_clamp_fusion), kind=kCustom, calls=%fused_computation | custom fusion | bytes 12589056 | tf_op jit(solution)/shard_map/jit(_take)/gather | solution.py:187
  28.8 1.8 dynamic-slice_select_fusion
  30.8 43.9 %all_to_all.20 = bf16[8,2,96,512]{3,2,1,0:T(8,128)(2,1)S(1)} all-to-all(bf16[8,2,96,512]{3,2,1,0:T(8,128)(2,1)S(1)} %fusion.47), channel_id=1, replica_groups=mesh['ep'=8,'tp'=4] {'ep'}, dimensions={0} | all-to-all | bytes 3145728 | tf_op jit(solution)/shard_map/all_to_all | solution.py:190
  74.7 1.3 copy.137
  76.1 0.7 slice.91
  76.8 0.7 slice.92
  77.5 1.0 copy.111
  78.6 2.2 collective-permute-start
  80.8 0.6 compare_select_fusion
  82.9 0.6 fusion.67
  84.5 1.3 mul.329
  85.8 1.0 slice.124
  86.8 2.9 fusion.39
  89.7 2.7 reshape.202
  92.4 1.0 fusion.65
  93.5 1.9 multiply_convert_fusion.2
  95.6 2.9 broadcast_multiply_fusion
  98.7 3.1 %fusion.26 = f32[2,16,64,128]{3,2,1,0:T(8,128)} fusion(f32[2,128,16,128]{3,1,2,0:T(8,128)S(1)} %bitcast.155, f32[2,128,16,64]{1,0,3,2:T(2,128)S(1)} %get-tuple-element.115), kind=kOutput, calls=%fused_computation.43 | convolution fusion | flops 402653184 | bytes 4194304 | tf_op jit(solution)/shard_map/bjhn,bjh,bjhp->bhpn/dot_general | solution.py:145
  101.8 4.1 %while.26 = (s32[]{:T(128)}, f32[16,64,128]{2,1,0:T(8,128)S(1)}, f32[2,16,64,128]{3,2,1,0:T(8,128)}, f32[2,16]{1,0:T(2,128)S(1)}, f32[2,16,64,128]{3,2,1,0:T(8,128)}, /*index=5*/s32[]{:T(128)}, s32[]{:T(128)}) while((s32[]{:T(128)}, f32[16,64,128]{2,1,0:T(8,128)S(1)}, f32[2,16,64,128]{3,2,1,0:T(8,128)}, f32[2,16]{1,0:T(2,128)S(1)}, ...), condition=%wide.region_2.3_spmd.clone, body=%wide.region_1.2_spmd.clone.sunk | while | flops 524291 | bytes 2622240 | solution.py:147
  101.8 0.9 bitcast_dynamic-update-slice_fusion.2
  102.7 1.2 bitcast_add_fusion.3
  103.8 0.9 bitcast_dynamic-update-slice_fusion.2
  104.7 1.2 bitcast_add_fusion.3
  105.9 0.7 convert_element_type.144
  106.9 38.1 %all-gather.9.cloned.1.call-done = bf16[2,768,2048]{2,1,0:T(8,128)(2,1)} async-done(((bf16[2,768,512]{2,1,0:T(8,128)(2,1)}), bf16[2,768,2048]{2,1,0:T(8,128)(2,1)}) %all-gather.9.cloned.1.call-update) | async-done | bytes 6291472 | tf_op jit(solution)/shard_map/all_gather | solution.py:193
  145.0 5.3 %fusion.70 = f32[2,768,256]{2,1,0:T(8,128)S(1)} fusion(bf16[2,768,2048]{2,1,0:T(8,128)(2,1)} %all-gather.9.cloned.1.call-done, bf16[2,2048,256]{2,1,0:T(8,128)(2,1)} %param.44), kind=kOutput, calls=%fused_computation.139 | convolution fusion | flops 1610612736 | bytes 9961472 | tf_op jit(solution)/shard_map/esd,edf->esf/dot_general | solution.py:194
  150.8 2.9 multiply_convert_fusion
  154.0 0.7 mul.373
  154.7 0.7 mul.368
  155.3 1.2 dynamic-slice
  157.5 17.2 %all-reduce.1 = bf16[128]{0:T(256)(128)(2,1)S(1)} all-reduce(bf16[128]{0:T(256)(128)(2,1)S(1)} %dynamic-update-slice), channel_id=2, replica_groups=mesh['ep'=8,'tp'=4] {'ep'}, use_global_device_ids=true, to_apply=%add.1 | all-reduce | flops 128 | bytes 512
  174.7 0.7 reshape.243
  175.3 0.7 copy.126
  176.1 1.1 copy.128
  177.1 0.6 iota_compare_fusion.2
  177.8 0.9 fusion.69
  179.2 0.8 copy.125
  180.4 1.4 broadcast_in_dim.92
  181.8 4.2 %fusion.16 = f32[2,128,16,64]{1,3,2,0:T(8,128)S(1)} fusion(f32[2,128,16,128]{3,1,2,0:T(8,128)S(1)} %bitcast.156, f32[2,16,64,128]{3,2,1,0:T(8,128)S(1)} %copy-done.9, f32[2,128,16]{1,2,0:T(8,128)S(1)} %copy-done.14, f32[16,64,128]{2,1,0:T(8,128)S(1)} %get-tuple-element.76, f32[2,16]{1,0:T(2,128)S(1)} %copy-done.33), kind=kOutput, calls=%fused_computation.27 | convolution fusion | flops 403439616 | bytes 4735104 | tf_op jit(solution)/shard_map/bihn,bhpn->bihp/dot_general | solution.py:159
  186.2 1.0 copy-done.6
  187.3 4.3 %fusion.13 = f32[2,128,16,64]{1,3,2,0:T(8,128)S(1)} fusion(f32[2,128,16,64]{1,3,2,0:T(8,128)S(1)} %fusion.16, f32[2,16,128,128]{3,2,1,0:T(8,128)S(1)} %bitcast.154, f32[2,128,16,64]{1,0,3,2:T(2,128)S(1)} %copy-done.6, f32[2,16,128]{2,1,0:T(8,128)S(1)} %copy.119, pred[128,128]{1,0:T(8,128)(4,1)S(1)} %copy-done.13), kind=kOutput, calls=%fused_computation.25 | convolution fusion | flops 405012480 | bytes 5275648 | tf_op jit(solution)/shard_map/bhij,bjhp->bihp/dot_general | solution.py:140
  191.5 1.8 copy.127
  193.3 3.1 %reshape.210 = f32[256,4,256]{0,2,1:T(8,128)} reshape(f32[2,128,16,64]{1,0,3,2:T(2,128)} %copy.127) | data formatting | bytes 2097152 | tf_op jit(solution)/shard_map/reshape | solution.py:162
  196.5 1.9 multiply_reduce_fusion.1
  198.4 1.3 fusion.25
  199.8 21.9 %all-gather.11.cloned.1.call-done = bf16[2,768,1024]{2,1,0:T(8,128)(2,1)} async-done(((bf16[2,768,256]{2,1,0:T(8,128)(2,1)}), bf16[2,768,1024]{2,1,0:T(8,128)(2,1)}) %all-gather.11.cloned.1.call-update) | async-done | bytes 3145744 | tf_op jit(solution)/shard_map/all_gather | solution.py:207
  221.7 3.7 %convolution_convert_fusion = bf16[2,768,512]{2,1,0:T(8,128)(2,1)S(1)} fusion(bf16[2,768,1024]{2,1,0:T(8,128)(2,1)} %all-gather.11.cloned.1.call-done, bf16[2,1024,512]{2,1,0:T(8,128)(2,1)S(1)} %copy-done), kind=kOutput, calls=%fused_computation.21 | convolution fusion | flops 1611399168 | bytes 6815744 | tf_op jit(solution)/shard_map/esf,efd->esd/dot_general | solution.py:213
  225.3 2.8 copy.138
  228.1 5.0 %all-to-all-start.1 = ((bf16[2,768,512]{2,0,1:T(2,128)(2,1)}), bf16[2,768,512]{2,0,1:T(2,128)(2,1)}, u32[]{:S(2)}, u32[]{:S(2)}) async-start(bf16[2,768,512]{2,0,1:T(2,128)(2,1)} %copy.138), calls=%async_computation.1 | async-start | bytes 3145728 | tf_op jit(solution)/shard_map/all_to_all | solution.py:216
  233.7 1.7 fusion.71
  235.9 20.6 %all_gather.28 = bf16[256,1024]{1,0:T(8,128)(2,1)} all-gather(bf16[256,256]{1,0:T(8,128)(2,1)S(1)} %fusion.18), channel_id=1, replica_groups=mesh['ep'=8,'tp'=4] {'tp'}, dimensions={1}, use_global_device_ids=true | all-gather | bytes 655360 | tf_op jit(solution)/shard_map/all_gather | solution.py:208
  256.5 6.2 %all-gather.7.cloned.1.call-done = bf16[256,4096]{0,1:T(8,128)(2,1)} async-done(((bf16[256,1024]{0,1:T(8,128)(2,1)}), bf16[256,4096]{0,1:T(8,128)(2,1)}) %all-gather.7.cloned.1.call-update) | async-done | bytes 2097168 | tf_op jit(solution)/shard_map/all_gather | solution.py:206
  262.8 4.8 %convolution_convert_fusion.1 = bf16[256,512]{1,0:T(8,128)(2,1)} fusion(bf16[256,4096]{0,1:T(8,128)(2,1)} %all-gather.7.cloned.1.call-done, bf16[4096,512]{1,0:T(8,128)(2,1)} %param.39), kind=kOutput, calls=%fused_computation.32 | convolution fusion | flops 1073872896 | bytes 6553600 | tf_op jit(solution)/shard_map/dot_general | solution.py:210
  267.5 3.4 %all-to-all-done.1 = bf16[2,768,512]{2,0,1:T(2,128)(2,1)} async-done(((bf16[2,768,512]{2,0,1:T(2,128)(2,1)}), bf16[2,768,512]{2,0,1:T(2,128)(2,1)}, u32[]{:S(2)}, u32[]{:S(2)}) %all-to-all-start.1) | async-done | bytes 1572896 | tf_op jit(solution)/shard_map/all_to_all | solution.py:216
  271.0 2.9 copy.139
  273.9 5.6 %gather_fusion.1 = bf16[1024,512]{1,0:T(8,128)(2,1)S(1)} fusion(bf16[1536,512]{1,0:T(8,128)(2,1)} %bitcast.151, s32[1024]{0:T(1024)S(1)} %broadcast_clamp_fusion), kind=kCustom, calls=%fused_computation.1 | custom fusion | bytes 2101248 | tf_op jit(solution)/shard_map/jit(_take)/gather | solution.py:217
  279.5 1.1 gather.15
  280.6 3.4 %multiply_reduce_fusion = f32[256,512]{1,0:T(8,128)S(1)} fusion(f32[256,4]{1,0:T(8,128)S(1)} %copy.140, bf16[256,4,512]{2,1,0:T(4,128)(2,1)} %gather.15, pred[256,4]{1,0:T(8,128)(4,1)S(1)} %copy.135), kind=kLoop, calls=%fused_computation.14 | loop fusion | flops 1966080 | bytes 1577984 | tf_op jit(solution)/shard_map/reduce_sum | solution.py:219
  284.0 2.2 fusion.17
  (161 shorter events, 9.5 us)
Async XLA Ops:
  7.2 214.5 %copy-start = (bf16[2,1024,512]{2,1,0:T(8,128)(2,1)S(1)}, bf16[2,1024,512]{2,1,0:T(8,128)(2,1)}, u32[]{:S(2)}) copy-start(bf16[2,1024,512]{2,1,0:T(8,128)(2,1)} %param.46) | copy-start | bytes 6291460
  7.2 12.8 %copy-start.7 = (bf16[256,2048]{1,0:T(8,128)(2,1)S(1)}, bf16[256,2048]{1,0:T(8,128)(2,1)}, u32[]{:S(2)}) copy-start(bf16[256,2048]{1,0:T(8,128)(2,1)} %param.40) | copy-start | bytes 3145732
  7.2 13.2 %copy-start.25 = (f32[2048]{0:T(1024)S(1)}, f32[2048]{0:T(1024)}, u32[]{:S(2)}) copy-start(f32[2048]{0:T(1024)} %param.41) | copy-start | bytes 24580
  7.2 137.8 %all-gather.9.cloned.1.call-start = ((), (), s32[]{:S(2)}) async-start(), calls=%async_computation.3 | async-start | bytes 7864320 | tf_op jit(solution)/shard_map/all_gather | solution.py:193
  14.4 0.6 copy-start.15
  15.0 0.6 copy-start.20
  20.7 1.0 copy-start.2
  74.7 1.4 copy-start.10
  74.7 6.0 %copy-start.40 = (f32[16]{0:T(128)S(1)}, f32[16]{0:T(128)}, u32[]{:S(2)}) copy-start(f32[16]{0:T(128)} %param.33) | copy-start | bytes 196
  74.7 6.0 %copy-start.23 = (f32[256,16]{0,1:T(8,128)S(1)}, f32[256,16]{0,1:T(8,128)}, u32[]{:S(2)}) copy-start(f32[256,16]{0,1:T(8,128)} %param.31) | copy-start | bytes 49156
  74.7 6.0 %copy-start.24 = (f32[256,16]{0,1:T(8,128)S(1)}, f32[256,16]{0,1:T(8,128)}, u32[]{:S(2)}) copy-start(f32[256,16]{0,1:T(8,128)} %param.32) | copy-start | bytes 49156
  76.0 6.3 %copy-start.30 = (f32[4,512]{1,0:T(4,128)S(1)}, f32[4,512]{1,0:T(4,128)}, u32[]{:S(2)}) copy-start(f32[4,512]{1,0:T(4,128)} %param.36) | copy-start | bytes 24580
  76.0 6.9 %copy-start.22 = (f32[4,1024]{1,0:T(4,128)S(1)}, f32[4,1024]{1,0:T(4,128)}, u32[]{:S(2)}) copy-start(f32[4,1024]{1,0:T(4,128)} %param.35) | copy-start | bytes 49156
  76.0 104.3 %all-gather.13.cloned.1.call-start = ((), (), s32[]{:S(2)}) async-start(), calls=%async_computation.5 | async-start | bytes 2359296 | tf_op jit(solution)/shard_map/all_gather | solution.py:24
  78.6 7.2 %collective-permute-start = (bf16[3,2048]{0,1:T(8,128)(2,1)}, bf16[3,2048]{0,1:T(8,128)(2,1)}, u32[]{:S(2)}, u32[]{:S(2)}) collective-permute-start(bf16[3,2048]{0,1:T(8,128)(2,1)} %copy.111), channel_id=1, source_target_pairs={{0,4},{4,8},{8,12},{12,16},{16,20},{20,24},{24,28},{1,5},{5,9},{9,... | collective-permute-start | bytes 36872 | tf_op jit(solution)/shard_map/ppermute | solution.py:18
  89.7 3.8 %copy-start.26 = (f32[1,512]{1,0:T(1,128)S(1)}, f32[1,512]{1,0:T(1,128)}, u32[]{:S(2)}) copy-start(f32[1,512]{1,0:T(1,128)} %get-tuple-element.129) | copy-start | bytes 6148
  89.7 3.8 %copy-start.27 = (f32[1,512]{1,0:T(1,128)S(1)}, f32[1,512]{1,0:T(1,128)}, u32[]{:S(2)}) copy-start(f32[1,512]{1,0:T(1,128)} %get-tuple-element.130) | copy-start | bytes 6148
  89.7 3.8 %copy-start.28 = (f32[1,512]{1,0:T(1,128)S(1)}, f32[1,512]{1,0:T(1,128)}, u32[]{:S(2)}) copy-start(f32[1,512]{1,0:T(1,128)} %get-tuple-element.131) | copy-start | bytes 6148
  89.7 3.8 %copy-start.29 = (f32[1,512]{1,0:T(1,128)S(1)}, f32[1,512]{1,0:T(1,128)}, u32[]{:S(2)}) copy-start(f32[1,512]{1,0:T(1,128)} %get-tuple-element.132) | copy-start | bytes 6148
  98.7 3.1 %copy-start.34 = (f32[2,16]{1,0:T(2,128)S(1)}, f32[2,16]{1,0:T(2,128)}, u32[]{:S(2)}) copy-start(f32[2,16]{1,0:T(2,128)} %get-tuple-element.205) | copy-start | bytes 388
  106.7 115.0 %all-gather.11.cloned.1.call-start = ((), (), s32[]{:S(2)}) async-start(), calls=%async_computation.4 | async-start | bytes 3932160 | tf_op jit(solution)/shard_map/all_gather | solution.py:207
  145.0 5.4 %copy-start.37 = (bf16[2,768,2048]{2,1,0:T(8,128)(2,1)S(1)}, bf16[2,768,2048]{2,1,0:T(8,128)(2,1)}, u32[]{:S(2)}) copy-start(bf16[2,768,2048]{2,1,0:T(8,128)(2,1)} %all-gather.9.cloned.1.call-done) | copy-start | bytes 18874372
  145.0 5.8 %copy-start.38 = (bf16[2,2048,256]{2,1,0:T(8,128)(2,1)S(1)}, bf16[2,2048,256]{2,1,0:T(8,128)(2,1)}, u32[]{:S(2)}) copy-start(bf16[2,2048,256]{2,1,0:T(8,128)(2,1)} %param.45) | copy-start | bytes 6291460
  150.8 3.0 %copy-start.35 = (f32[16]{0:T(128)S(1)}, f32[16]{0:T(128)}, u32[]{:S(2)}) copy-start(f32[16]{0:T(128)} %param.34) | copy-start | bytes 196
  150.8 6.4 %copy-start.36 = (f32[16]{0:T(128)S(1)}, f32[16]{0:T(128)}, u32[]{:S(2)}) copy-start(f32[16]{0:T(128)} %get-tuple-element.119) | copy-start | bytes 196
  150.8 25.2 %copy-start.11 = (bf16[256,1024]{1,0:T(8,128)(2,1)S(1)}, bf16[256,1024]{1,0:T(8,128)(2,1)}, u32[]{:S(2)}) copy-start(bf16[256,1024]{1,0:T(8,128)(2,1)} %param.30) | copy-start | bytes 1572868
  153.8 25.0 %copy-start.12 = (bf16[256,512]{1,0:T(8,128)(2,1)S(1)}, bf16[256,512]{1,0:T(8,128)(2,1)}, u32[]{:S(2)}) copy-start(bf16[256,512]{1,0:T(8,128)(2,1)} %param.29) | copy-start | bytes 786436
  153.8 109.0 %all-gather.7.cloned.1.call-start = ((), (), s32[]{:S(2)}) async-start(), calls=%async_computation.2 | async-start | bytes 2621440 | tf_op jit(solution)/shard_map/all_gather | solution.py:206
  180.4 1.4 copy-start.9
  180.4 1.4 copy-start.14
  180.4 1.4 copy-start.33
  186.0 1.3 copy-start.6
  186.0 1.3 copy-start.13
  191.5 4.9 %copy-start.1 = (f32[256,1024]{0,1:T(8,128)S(1)}, f32[256,1024]{0,1:T(8,128)}, u32[]{:S(2)}) copy-start(f32[256,1024]{0,1:T(8,128)} %fusion.39) | copy-start | bytes 3145732
  191.5 4.9 %copy-start.19 = (f32[4,256]{1,0:T(4,128)S(1)}, f32[4,256]{1,0:T(4,128)}, u32[]{:S(2)}) copy-start(f32[4,256]{1,0:T(4,128)} %mul.373) | copy-start | bytes 12292
  193.3 5.1 %copy-start.18 = (f32[1024]{0:T(1024)S(1)}, f32[1024]{0:T(1024)}, u32[]{:S(2)}) copy-start(f32[1024]{0:T(1024)} %mul.368) | copy-start | bytes 12292
  193.3 5.1 %copy-start.31 = (f32[1024]{0:T(1024)S(1)}, f32[1024]{0:T(1024)}, u32[]{:S(2)}) copy-start(f32[1024]{0:T(1024)} %param.38) | copy-start | bytes 12292
  196.5 2.0 copy-start.4
  196.5 2.0 copy-start.5
  228.1 5.0 %copy-start.16 = (s32[1024]{0:T(1024)S(1)}, s32[1024]{0:T(1024)}, u32[]{:S(2)}) copy-start(s32[1024]{0:T(1024)} %copy-done.15) | copy-start | bytes 12292
  228.1 5.2 %copy-start.17 = (s32[256,4]{0,1:T(4,128)S(1)}, s32[256,4]{0,1:T(4,128)}, u32[]{:S(2)}) copy-start(s32[256,4]{0,1:T(4,128)} %param.42) | copy-start | bytes 12292
  228.1 5.4 %copy-start.32 = (f32[256,4]{0,1:T(4,128)S(1)}, f32[256,4]{0,1:T(4,128)}, u32[]{:S(2)}) copy-start(f32[256,4]{0,1:T(4,128)} %param.43) | copy-start | bytes 12292
  228.1 5.5 %copy-start.3 = (bf16[256,2048]{1,0:T(8,128)(2,1)S(1)}, bf16[256,2048]{1,0:T(8,128)(2,1)}, u32[]{:S(2)}) copy-start(bf16[256,2048]{1,0:T(8,128)(2,1)} %copy-done.2) | copy-start | bytes 3145732
  228.1 42.9 %all-to-all-start.1 = ((bf16[2,768,512]{2,0,1:T(2,128)(2,1)}), bf16[2,768,512]{2,0,1:T(2,128)(2,1)}, u32[]{:S(2)}, u32[]{:S(2)}) async-start(bf16[2,768,512]{2,0,1:T(2,128)(2,1)} %copy.138), calls=%async_computation.1 | async-start | bytes 3145728 | tf_op jit(solution)/shard_map/all_to_all | solution.py:216
  233.7 1.8 copy-start.39
  235.4 21.1 %copy-start.21 = (s32[1024,1]{0,1:T(1,128)S(1)}, s32[1024,1]{0,1:T(1,128)}, u32[]{:S(2)}) copy-start(s32[1024,1]{0,1:T(1,128)} %copy-done.20) | copy-start | bytes 12292
  280.6 3.4 %copy-start.8 = (bf16[1024,512]{1,0:T(8,128)(2,1)S(1)}, bf16[1024,512]{1,0:T(8,128)(2,1)}, u32[]{:S(2)}) copy-start(bf16[1024,512]{1,0:T(8,128)(2,1)} %param.49) | copy-start | bytes 3145732
Sparse Core Ops, SparseCore 0:
  76.2 68.8 all-gather.8
  147.2 29.4 all-gather.12
  178.5 43.0 all-gather.10
  223.4 39.3 all-gather.6
